TPU v7x, 32 devices: a whole 2x2x4 slice. The times are simulated.
32 devices in a mesh: sp: 8 (over z, x), tp: 4 (over y, core).
Axes of the slice: x: 2, y: 2, z: 4, core: 2. Of those that a mesh axis runs over, the one named last changes fastest.
Arguments:
- skip_stream_input: bfloat16 [1024, 2048], P('sp'), may hold values from -16 to 16
- asking_vectors_split: bfloat16 [1024, 2048], P('sp', 'tp'), may hold values from -8 to 8
- lookup_vectors_split: bfloat16 [1024, 512], P('sp'), may hold values from -8 to 8
- content_vectors_split: bfloat16 [1024, 512], P('sp'), may hold values from -6 to 6
- asking_rms_gain: float32 [128], replicated, may hold values from 0.1 to 1.9
- lookup_rms_gain: float32 [128], replicated, may hold values from 0.1 to 1.9
- softness_per_channel: float32 [16], P('tp'), may hold values from 1.5 to 24
- mixing_exit_weights: bfloat16 [2048, 2048], P('tp'), may hold values from -0.125 to 0.125
- specialist_rms_gain: float32 [2048], replicated, may hold values from 0.1 to 1.9
- selected_dispatch_weights: float32 [1024, 2], P('sp'), may hold values from -6 to 6
- selected_specialist_ids: int32 [1024, 2], P('sp'), may hold values from 0 to 7, all different within a row; in each aligned block of 128 rows (0 to 127, 128 to 255, ...) at most 48 rows name the same one
- specialist_switch_weights: bfloat16 [8, 2048, 2048], P('sp', None, 'tp'), may hold values from -0.125 to 0.125
- specialist_widen_weights: bfloat16 [8, 2048, 2048], P('sp', None, 'tp'), may hold values from -0.125 to 0.125
- specialist_shrink_weights: bfloat16 [8, 2048, 2048], P('sp', 'tp'), may hold values from -0.125 to 0.125
Outputs:
- layer_out: bfloat16 [1024, 2048], P('sp', 'tp')
Inputs may be any that keep to these rules, and one draw needn't show every extreme that they name: `selected_specialist_ids`: each row names 2 different experts. In each aligned block of 128 rows no expert is named by more than 48 rows, a bound that some block reaches.
All inputs are finite; a program needn't handle non-finite values.
Results may differ from a plain program's by a relative error of at most 0.0085.
Values may be sent and summed in bfloat16 or wider, within the bound.
A program may use at most 64 MiB of HBM per device.

v0:
```python
import math
import jax
import jax.numpy as jnp
from jax import lax
from jax.sharding import PartitionSpec as P

CHANNEL_WIDTH = 128
GROUP = 4
GRID_W = 64
EPSILON = 1e-06
NEGATIVE = -1e30


def rotate_half(values_in, positions, full_width):
    half_width = full_width // 2
    frequency = 10000.0 ** (-jnp.arange(half_width, dtype=jnp.float32) / half_width)
    angles = positions.astype(jnp.float32)[:, None] * frequency[None, :]
    cosine = jnp.cos(angles)[:, None, :]
    sine = jnp.sin(angles)[:, None, :]
    leading = values_in[..., :half_width]
    trailing = values_in[..., half_width:]
    return jnp.concatenate(
        [leading * cosine - trailing * sine, trailing * cosine + leading * sine], axis=-1
    )


def norm_rotate(heads_in, gain_vec, positions):
    widened = heads_in.astype(jnp.float32)
    scaled = (
        widened
        * lax.rsqrt(jnp.mean(widened * widened, axis=-1, keepdims=True) + EPSILON)
        * gain_vec
    )
    half_width = scaled.shape[-1] // 2
    grid_rows = positions // GRID_W
    grid_cols = positions % GRID_W
    turned = jnp.concatenate(
        [
            rotate_half(scaled[..., :half_width], grid_rows, half_width),
            rotate_half(scaled[..., half_width:], grid_cols, half_width),
        ],
        axis=-1,
    )
    return turned.astype(jnp.bfloat16)


def shards(
    skip_stream_input,
    asking_vectors_split,
    lookup_vectors_split,
    content_vectors_split,
    asking_rms_gain,
    lookup_rms_gain,
    softness_per_channel,
    mixing_exit_weights,
    specialist_rms_gain,
    selected_dispatch_weights,
    selected_specialist_ids,
    specialist_switch_weights,
    specialist_widen_weights,
    specialist_shrink_weights,
):
    tok_count = skip_stream_input.shape[0]
    model_width = skip_stream_input.shape[1]
    heads_here = asking_vectors_split.shape[1] // CHANNEL_WIDTH
    local_key_value_heads = max(1, heads_here // GROUP)
    local_group_count = heads_here // local_key_value_heads
    tp_position = lax.axis_index("tp")
    positions = lax.axis_index("sp") * tok_count + jnp.arange(tok_count, dtype=jnp.int32)
    query_turned = norm_rotate(
        asking_vectors_split.reshape(tok_count, heads_here, CHANNEL_WIDTH),
        asking_rms_gain,
        positions,
    )
    first_head = tp_position * heads_here // GROUP
    key_cols = lax.dynamic_slice_in_dim(
        lookup_vectors_split, first_head * CHANNEL_WIDTH, local_key_value_heads * CHANNEL_WIDTH, 1
    )
    value_cols = lax.dynamic_slice_in_dim(
        content_vectors_split, first_head * CHANNEL_WIDTH, local_key_value_heads * CHANNEL_WIDTH, 1
    )
    key_turned = norm_rotate(
        key_cols.reshape(tok_count, local_key_value_heads, CHANNEL_WIDTH),
        lookup_rms_gain,
        positions,
    )
    key_turned = key_turned.reshape(tok_count, local_key_value_heads * CHANNEL_WIDTH)
    query_grouped = query_turned.reshape(
        tok_count, local_key_value_heads, local_group_count, CHANNEL_WIDTH
    ).transpose(1, 2, 0, 3)
    inverse_root_width = (softness_per_channel / math.sqrt(CHANNEL_WIDTH)).reshape(
        local_key_value_heads, local_group_count, 1, 1
    )

    def absorb(run_state, key_span, value_span):
        run_max, run_sum, run_acc = run_state
        scores = (
            jnp.einsum(
                "kgqd,nkd->kgqn", query_grouped, key_span, preferred_element_type=jnp.float32
            )
            * inverse_root_width
        )
        new_max = jnp.maximum(run_max, jnp.max(scores, axis=-1))
        factor = jnp.exp(run_max - new_max)
        exp_terms = jnp.exp(scores - new_max[..., None])
        run_sum = run_sum * factor + jnp.sum(exp_terms, axis=-1)
        run_acc = run_acc * factor[..., None] + jnp.einsum(
            "kgqn,nkd->kgqd",
            exp_terms.astype(jnp.bfloat16),
            value_span,
            preferred_element_type=jnp.float32,
        )
        return (new_max, run_sum, run_acc)

    initial = (
        jnp.full((local_key_value_heads, local_group_count, tok_count), NEGATIVE, jnp.float32),
        jnp.zeros((local_key_value_heads, local_group_count, tok_count), jnp.float32),
        jnp.zeros(
            (local_key_value_heads, local_group_count, tok_count, CHANNEL_WIDTH), jnp.float32
        ),
    )
    key_piece = lax.all_gather(key_turned, "sp", axis=0, tiled=True)
    value_piece = lax.all_gather(value_cols, "sp", axis=0, tiled=True)
    piece_len = key_piece.shape[0]
    span_len = 1024
    span_count = piece_len // span_len
    key_spans = key_piece.reshape(span_count, span_len, local_key_value_heads, CHANNEL_WIDTH)
    value_spans = value_piece.reshape(span_count, span_len, local_key_value_heads, CHANNEL_WIDTH)

    def step_span(inner_state, span_pair):
        return (absorb(inner_state, span_pair[0], span_pair[1]), None)

    result_state, unused = lax.scan(step_span, initial, (key_spans, value_spans))
    final_max, final_sum, final_acc = result_state
    attn_heads = (final_acc / final_sum[..., None]).astype(jnp.bfloat16)
    attn_flat = attn_heads.transpose(2, 0, 1, 3).reshape(tok_count, heads_here * CHANNEL_WIDTH)
    partial_sum = jnp.dot(attn_flat, mixing_exit_weights, preferred_element_type=jnp.float32)
    share_width = model_width // lax.axis_size("tp")
    first_col = tp_position * share_width
    attended = lax.psum(partial_sum.astype(jnp.bfloat16), "tp")
    mid_rows = (skip_stream_input.astype(jnp.float32) + attended.astype(jnp.float32)).astype(
        jnp.bfloat16
    )
    mid_wide = mid_rows.astype(jnp.float32)
    normed_rows = (
        mid_wide
        * lax.rsqrt(jnp.mean(mid_wide * mid_wide, axis=-1, keepdims=True) + EPSILON)
        * specialist_rms_gain
    ).astype(jnp.bfloat16)
    mid_share = lax.dynamic_slice_in_dim(mid_rows, first_col, share_width, 1)
    outgoing_rows = lax.dynamic_slice_in_dim(normed_rows, first_col, share_width, 1)
    experts_count = lax.axis_size("sp")
    top_count = selected_specialist_ids.shape[1]
    capacity = max(2, 3 * tok_count * top_count // (2 * experts_count))
    flat_ids = selected_specialist_ids.reshape(-1)
    one_hot = (flat_ids[:, None] == jnp.arange(experts_count, dtype=jnp.int32)[None, :]).astype(
        jnp.int32
    )
    earlier = jnp.cumsum(one_hot, axis=0) - one_hot
    slot_index = jnp.sum(earlier * one_hot, axis=1)
    destination = flat_ids * capacity + slot_index
    owner_rows = jnp.arange(tok_count * top_count, dtype=jnp.int32) // top_count
    slot_owner = jnp.zeros((experts_count * capacity,), jnp.int32).at[destination].set(owner_rows)
    filled = jnp.zeros((experts_count * capacity,), jnp.int32).at[destination].set(1)
    outgoing = jnp.where(
        filled[:, None] > 0, outgoing_rows[slot_owner], jnp.zeros((), jnp.bfloat16)
    )
    outgoing = outgoing.reshape(experts_count, capacity, outgoing_rows.shape[1])
    gate_local = specialist_switch_weights[0]
    up_local = specialist_widen_weights[0]
    down_local = specialist_shrink_weights[0]
    arrived = lax.all_to_all(outgoing, "sp", split_axis=0, concat_axis=0, tiled=True)
    row_count = arrived.shape[0] * arrived.shape[1]
    feature_piece = lax.all_gather(arrived, "tp", axis=2, tiled=True)
    piece_width = feature_piece.shape[2]
    flat_piece = feature_piece.reshape(row_count, piece_width)
    gate_acc = jnp.dot(flat_piece, gate_local, preferred_element_type=jnp.float32)
    up_acc = jnp.dot(flat_piece, up_local, preferred_element_type=jnp.float32)
    hidden = (jax.nn.silu(gate_acc) * up_acc).astype(jnp.bfloat16)
    expert_part = jnp.dot(hidden, down_local, preferred_element_type=jnp.float32)
    expert_part = expert_part.reshape(arrived.shape[0], arrived.shape[1], model_width)
    expert_share = lax.psum_scatter(
        expert_part.astype(jnp.bfloat16), "tp", scatter_dimension=2, tiled=True
    )
    returned = lax.all_to_all(expert_share, "sp", split_axis=0, concat_axis=0, tiled=True)
    back_flat = returned.reshape(experts_count * capacity, share_width)
    picked = back_flat[destination].reshape(tok_count, top_count, share_width).astype(jnp.float32)
    route_weights = jax.nn.softmax(selected_dispatch_weights, axis=-1)
    layer_out = mid_share.astype(jnp.float32) + jnp.sum(route_weights[..., None] * picked, axis=1)
    return layer_out.astype(jnp.bfloat16)


def solution(mesh):
    in_specs = (
        P("sp", None),
        P("sp", "tp"),
        P("sp", None),
        P("sp", None),
        P(),
        P(),
        P("tp"),
        P("tp", None),
        P(),
        P("sp", None),
        P("sp", None),
        P("sp", None, "tp"),
        P("sp", None, "tp"),
        P("sp", "tp", None),
    )
    out_specs = P("sp", "tp")
    return jax.shard_map(shards, mesh=mesh, in_specs=in_specs, out_specs=out_specs, check_vma=False)
```

profile of v0, /device:TPU:0, one launch (start us, length us, event | category | flops | bytes accessed | tf_op | source)
XLA Modules:
  0.0 204.7 jit_solution(4723165117829957611)
XLA Ops:
  6.6 0.9 constant_dynamic-slice_fusion.1
  9.2 28.3 %all_gather.9 = bf16[1024,128]{0,1:T(8,128)(2,1)S(1)} all-gather(bf16[128,128]{0,1:T(8,128)(2,1)S(1)} %pad_maximum_fusion), channel_id=1, replica_groups=mesh['sp'=8,'tp'=4] {'sp'}, dimensions={0}, use_global_device_ids=true | all-gather | bytes 294912 | tf_op jit(solution)/shard_map/all_gather | solution.py:122
  37.5 1.0 copy.24
  39.4 0.8 multiply_multiply_fusion
  41.1 1.3 copy-done.1
  42.9 0.8 constant_dynamic-slice_fusion
  43.8 26.8 %all_gather.10 = bf16[1024,128]{0,1:T(8,128)(2,1)S(1)} all-gather(bf16[128,128]{0,1:T(8,128)(2,1)S(1)} %copy.36), channel_id=1, replica_groups=mesh['sp'=8,'tp'=4] {'sp'}, dimensions={0}, use_global_device_ids=true | all-gather | bytes 294912 | tf_op jit(solution)/shard_map/all_gather | solution.py:123
  70.7 2.2 %fusion.14 = bf16[4,128,128]{1,2,0:T(8,128)(2,1)S(1)} fusion(f32[4,128,1024]{2,1,0:T(8,128)} %copy-done.1, f32[4,128]{1,0:T(4,128)S(1)} %broadcast_maximum_fusion, f32[4]{0:T(128)S(1)} %broadcast_multiply_fusion.1, bf16[1024,128]{0,1:T(8,128)(2,1)S(1)} %all_gather.10, f32[4,128]{1,0:T(4,128)S(1)} %get-tuple-element.44, f32[4,128]{1,0:T(4,128)S(1)} %get-tuple-element.43), kind=kOutput, calls=%fused_computation.19 | convolution fusion | flops 135987200 | bytes 2496528 | tf_op jit(solution)/shard_map/while/body/eval_jaxpr/kgqn,nkd->kgqd/dot_general | solution.py:107
  72.9 1.3 convolution_convert_fusion.1
  75.9 1.4 scatter_custom_fusion.1
  77.3 1.4 scatter_custom_fusion
  78.8 0.8 dynamic-slice
  79.6 25.8 %all-reduce.2.cloned.1.call-done = bf16[128,2048]{1,0:T(8,128)(2,1)} async-done(((bf16[128,2048]{1,0:T(8,128)(2,1)}), bf16[128,2048]{1,0:T(8,128)(2,1)}) %all-reduce.2.cloned.1.call-update) | async-done | bytes 524304 | tf_op jit(solution)/shard_map/psum | solution.py:140
  105.4 1.3 multiply_reduce_fusion.1
  106.9 2.1 %gather_fusion = bf16[384,512]{1,0:T(8,128)(2,1)S(1)} fusion(bf16[128,512]{1,0:T(8,128)(2,1)S(1)} %fusion.19, s32[1024]{0:T(1024)S(1)} %pad_clamp_fusion.1), kind=kCustom, calls=%fused_computation | custom fusion | bytes 787968 | tf_op jit(solution)/shard_map/gather | solution.py:166
  109.1 16.5 %all_to_all.10 = bf16[8,48,512]{2,1,0:T(8,128)(2,1)} all-to-all(bf16[8,48,512]{2,1,0:T(8,128)(2,1)S(1)} %broadcast_select_fusion), channel_id=1, replica_groups=mesh['sp'=8,'tp'=4] {'sp'}, dimensions={0} | all-to-all | bytes 786432 | tf_op jit(solution)/shard_map/all_to_all | solution.py:172
  125.7 18.0 %all-gather.2.cloned.1.call-done = bf16[8,48,2048]{2,1,0:T(8,128)(2,1)} async-done(((bf16[8,48,512]{2,1,0:T(8,128)(2,1)}), bf16[8,48,2048]{2,1,0:T(8,128)(2,1)}) %all-gather.2.cloned.1.call-update) | async-done | bytes 1572880 | tf_op jit(solution)/shard_map/all_gather | solution.py:174
  143.7 3.2 %fusion.3 = f32[384,512]{1,0:T(8,128)S(1)} fusion(bf16[384,2048]{1,0:T(8,128)(2,1)} %bitcast.82, bf16[1,2048,512]{2,1,0:T(8,128)(2,1)} %param.25), kind=kOutput, calls=%fused_computation.9 | convolution fusion | flops 805306368 | bytes 4456448 | tf_op jit(solution)/shard_map/dot_general | solution.py:177
  146.9 1.0 fusion.10
  147.9 2.1 %convolution_convert_fusion = bf16[8,48,2048]{2,1,0:T(8,128)(2,1)} fusion(bf16[8,48,512]{2,1,0:T(8,128)(2,1)S(1)} %bitcast.84, bf16[1,512,2048]{2,1,0:T(8,128)(2,1)S(1)} %copy-done), kind=kOutput, calls=%fused_computation.4 | convolution fusion | flops 806092800 | bytes 4063232 | tf_op jit(solution)/shard_map/dot_general | solution.py:180
  150.1 28.1 %reduce-scatter.2.cloned.1.call-done = bf16[8,48,512]{2,1,0:T(8,128)(2,1)} async-done(((bf16[8,48,2048]{2,1,0:T(8,128)(2,1)}), bf16[8,48,512]{2,1,0:T(8,128)(2,1)}) %reduce-scatter.2.cloned.1.call-update) | async-done | bytes 393232 | tf_op jit(solution)/shard_map/reduce_scatter | solution.py:182
  178.2 5.5 %all-to-all-start.1 = ((bf16[8,48,512]{2,1,0:T(8,128)(2,1)}), bf16[8,48,512]{2,1,0:T(8,128)(2,1)S(1)}, u32[]{:S(2)}, u32[]{:S(2)}) async-start(bf16[8,48,512]{2,1,0:T(8,128)(2,1)} %reduce-scatter.2.cloned.1.call-done), calls=%async_computation.2 | async-start | bytes 786432 | tf_op jit(solution)/shard_map/all_to_all | solution.py:185
  183.9 11.4 %all-to-all-done.1 = bf16[8,48,512]{2,1,0:T(8,128)(2,1)S(1)} async-done(((bf16[8,48,512]{2,1,0:T(8,128)(2,1)}), bf16[8,48,512]{2,1,0:T(8,128)(2,1)S(1)}, u32[]{:S(2)}, u32[]{:S(2)}) %all-to-all-start.1) | async-done | bytes 393248 | tf_op jit(solution)/shard_map/all_to_all | solution.py:185
  195.3 1.2 gather_fusion.1
  (71 shorter events, 8.1 us)
Async XLA Ops:
  6.5 141.4 %copy-start = (bf16[1,512,2048]{2,1,0:T(8,128)(2,1)S(1)}, bf16[1,512,2048]{2,1,0:T(8,128)(2,1)}, u32[]{:S(2)}) copy-start(bf16[1,512,2048]{2,1,0:T(8,128)(2,1)} %param.27) | copy-start | bytes 6291460
  6.5 98.8 %all-reduce.2.cloned.1.call-start = ((), (), s32[]{:S(2)}) async-start(), calls=%async_computation.3 | async-start | bytes 1048576 | tf_op jit(solution)/shard_map/psum | solution.py:140
  41.1 1.4 copy-start.1
  43.8 29.1 %copy-start.2 = (bf16[512,2048]{1,0:T(8,128)(2,1)S(1)}, bf16[512,2048]{1,0:T(8,128)(2,1)}, u32[]{:S(2)}) copy-start(bf16[512,2048]{1,0:T(8,128)(2,1)} %param.21) | copy-start | bytes 6291460
  72.9 1.4 copy-start.5
  72.9 32.5 %copy-start.3 = (bf16[128,2048]{1,0:T(8,128)(2,1)S(1)}, bf16[128,2048]{1,0:T(8,128)(2,1)}, u32[]{:S(2)}) copy-start(bf16[128,2048]{1,0:T(8,128)(2,1)} %param.14) | copy-start | bytes 1572868
  74.2 69.4 %all-gather.2.cloned.1.call-start = ((), (), s32[]{:S(2)}) async-start(), calls=%async_computation.4 | async-start | bytes 1966080 | tf_op jit(solution)/shard_map/all_gather | solution.py:174
  125.6 52.6 %reduce-scatter.2.cloned.1.call-start = ((), (), s32[]{:S(2)}) async-start(), calls=%async_computation.5 | async-start | bytes 1966080 | tf_op jit(solution)/shard_map/reduce_scatter | solution.py:182
  143.7 3.2 %copy-start.6 = (bf16[1,2048,512]{2,1,0:T(8,128)(2,1)S(1)}, bf16[1,2048,512]{2,1,0:T(8,128)(2,1)}, u32[]{:S(2)}) copy-start(bf16[1,2048,512]{2,1,0:T(8,128)(2,1)} %param.26) | copy-start | bytes 6291460
  143.7 3.2 %copy-start.7 = (bf16[8,48,2048]{2,1,0:T(8,128)(2,1)S(1)}, bf16[8,48,2048]{2,1,0:T(8,128)(2,1)}, u32[]{:S(2)}) copy-start(bf16[8,48,2048]{2,1,0:T(8,128)(2,1)} %all-gather.2.cloned.1.call-done) | copy-start | bytes 4718596
  150.0 33.7 %copy-start.4 = (f32[128,2]{0,1:T(2,128)S(1)}, f32[128,2]{0,1:T(2,128)}, u32[]{:S(2)}) copy-start(f32[128,2]{0,1:T(2,128)} %param.23) | copy-start | bytes 3076
  178.2 17.1 %all-to-all-start.1 = ((bf16[8,48,512]{2,1,0:T(8,128)(2,1)}), bf16[8,48,512]{2,1,0:T(8,128)(2,1)S(1)}, u32[]{:S(2)}, u32[]{:S(2)}) async-start(bf16[8,48,512]{2,1,0:T(8,128)(2,1)} %reduce-scatter.2.cloned.1.call-done), calls=%async_computation.2 | async-start | bytes 786432 | tf_op jit(solution)/shard_map/all_to_all | solution.py:185
Sparse Core Ops, SparseCore 0:
  74.3 30.9 all-reduce.1
  125.8 17.8 all-gather.1
  150.2 27.9 reduce-scatter.1
where the time goes:
time: 205 us
  waiting for transfers between devices  83.3 us (41%)
  blocking collectives  71.7 us (35%)
  between operations  13.5 us (7%)
  local copies, waits for them, and re-layouts  12.6 us (6%)
  matrix products  10.4 us (5%)
  other arithmetic  7.66 us (4%)
  starting transfers between devices  5.57 us (3%)
    all_gather x1, blocking collectives, shards(): key_piece = lax.all_gather(key_turned, 'sp', axis=0, tiled=True)  28.3 us
    reduce_scatter x1, waiting for transfers between devices, shards(): lax.psum_scatter(expert_part.astype(jnp.bfloat16), 'tp', scatter_dimensio...  28.1 us
    all_gather x1, blocking collectives, shards(): value_piece = lax.all_gather(value_cols, 'sp', axis=0, tiled=True)  26.8 us
    psum x1, waiting for transfers between devices, shards(): attended = lax.psum(partial_sum.astype(jnp.bfloat16), 'tp')  25.8 us
    all_gather x1, waiting for transfers between devices, shards(): feature_piece = lax.all_gather(arrived, 'tp', axis=2, tiled=True)  18 us
    all_to_all x1, blocking collectives, shards(): lax.all_to_all(outgoing, 'sp', split_axis=0, concat_axis=0, tiled=True)  16.5 us
    all_to_all x1, waiting for transfers between devices, shards(): lax.all_to_all(expert_share, 'sp', split_axis=0, concat_axis=0, tiled=True)  11.4 us
    all_to_all x1, starting transfers between devices, shards(): lax.all_to_all(expert_share, 'sp', split_axis=0, concat_axis=0, tiled=True)  5.48 us
  transfers between devices with their start and end apart: 4, of which 4 were waited for; matrix products, arithmetic and copies ran while one was open for 3% of the time, Pallas kernels for 0%

commit v1 on v0

--- a/solution.py
+++ b/solution.py
@@ -171,7 +171,9 @@
     down_local = specialist_shrink_weights[0]
     arrived = lax.all_to_all(outgoing, "sp", split_axis=0, concat_axis=0, tiled=True)
     row_count = arrived.shape[0] * arrived.shape[1]
-    feature_piece = lax.all_gather(arrived, "tp", axis=2, tiled=True)
+    feature_piece = jnp.concatenate(
+        lax.all_to_all(jnp.stack([arrived] * lax.axis_size("tp")), "tp", 0, 0), axis=2
+    )
     piece_width = feature_piece.shape[2]
     flat_piece = feature_piece.reshape(row_count, piece_width)
     gate_acc = jnp.dot(flat_piece, gate_local, preferred_element_type=jnp.float32)

time: 205 us -> 209 us (1.020)
  blocking collectives: 71.7 us -> 94.1 us
  waiting for transfers between devices: 83.3 us -> 63.1 us
  local copies, waits for them, and re-layouts: 12.6 us -> 16.2 us
  matrix products: 10.4 us -> 8.19 us
    all_to_all x0 -> x1, blocking collectives: none -> 22.5 us  [shards(): lax.all_to_all(jnp.stack([arrived] * lax.axis_size('tp')), 'tp', 0, 0)]
    all_gather x1 -> x0, waiting for transfers between devices: 18 us -> none  [shards(): feature_piece = lax.all_gather(arrived, 'tp', axis=2, tiled=True)]
    reduce_scatter x1, waiting for transfers between devices: 28.1 us -> 25.9 us  [shards(): lax.psum_scatter(expert_part.astype(jnp.bfloat16), 'tp', scatter_dimensio...]
    dot_general x1, matrix products: 3.18 us -> 0.97 us  [shards(): jnp.dot(flat_piece, gate_local, preferred_element_type=jnp.float32)]
    unnamed x20 -> x21, local copies, waits for them, and re-layouts: 2.73 us -> 4.92 us
  transfers between devices with their start and end apart: 4 -> 3, of which waited for: 4 -> 3; matrix products, arithmetic and copies ran while one was open for 3% -> 3% of each run, Pallas kernels for 0% -> 0%
where the time goes in v1:
time: 209 us
  blocking collectives  94.1 us (45%)
  waiting for transfers between devices  63.1 us (30%)
  local copies, waits for them, and re-layouts  16.2 us (8%)
  between operations  13.8 us (7%)
  matrix products  8.19 us (4%)
  other arithmetic  7.66 us (4%)
  starting transfers between devices  5.57 us (3%)
    all_gather x1, blocking collectives, shards(): key_piece = lax.all_gather(key_turned, 'sp', axis=0, tiled=True)  28.3 us
    all_gather x1, blocking collectives, shards(): value_piece = lax.all_gather(value_cols, 'sp', axis=0, tiled=True)  26.8 us
    reduce_scatter x1, waiting for transfers between devices, shards(): lax.psum_scatter(expert_part.astype(jnp.bfloat16), 'tp', scatter_dimensio...  25.9 us
    psum x1, waiting for transfers between devices, shards(): attended = lax.psum(partial_sum.astype(jnp.bfloat16), 'tp')  25.8 us
    all_to_all x1, blocking collectives, shards(): lax.all_to_all(jnp.stack([arrived] * lax.axis_size('tp')), 'tp', 0, 0)  22.5 us
    all_to_all x1, blocking collectives, shards(): lax.all_to_all(outgoing, 'sp', split_axis=0, concat_axis=0, tiled=True)  16.4 us
    all_to_all x1, waiting for transfers between devices, shards(): lax.all_to_all(expert_share, 'sp', split_axis=0, concat_axis=0, tiled=True)  11.4 us
    all_to_all x1, starting transfers between devices, shards(): lax.all_to_all(expert_share, 'sp', split_axis=0, concat_axis=0, tiled=True)  5.53 us
  transfers between devices with their start and end apart: 3, of which 3 were waited for; matrix products, arithmetic and copies ran while one was open for 3% of the time, Pallas kernels for 0%

profile of v1, /device:TPU:0, one launch (start us, length us, event | category | flops | bytes accessed | tf_op | source)
XLA Modules:
  0.0 208.5 jit_solution(7177825886643292036)
XLA Ops:
  6.6 0.9 constant_dynamic-slice_fusion.1
  9.2 28.3 %all_gather.6 = bf16[1024,128]{0,1:T(8,128)(2,1)S(1)} all-gather(bf16[128,128]{0,1:T(8,128)(2,1)S(1)} %pad_maximum_fusion), channel_id=1, replica_groups=mesh['sp'=8,'tp'=4] {'sp'}, dimensions={0}, use_global_device_ids=true | all-gather | bytes 294912 | tf_op jit(solution)/shard_map/all_gather | solution.py:122
  37.5 1.0 copy.32
  39.4 0.8 multiply_multiply_fusion
  41.1 1.3 copy-done.1
  43.8 26.8 %all_gather.7 = bf16[1024,128]{0,1:T(8,128)(2,1)S(1)} all-gather(bf16[128,128]{0,1:T(8,128)(2,1)S(1)} %copy.45), channel_id=1, replica_groups=mesh['sp'=8,'tp'=4] {'sp'}, dimensions={0}, use_global_device_ids=true | all-gather | bytes 294912 | tf_op jit(solution)/shard_map/all_gather | solution.py:123
  70.7 2.2 %fusion.14 = bf16[4,128,128]{1,2,0:T(8,128)(2,1)S(1)} fusion(f32[4,128,1024]{2,1,0:T(8,128)} %copy-done.1, f32[4,128]{1,0:T(4,128)S(1)} %broadcast_maximum_fusion, f32[4]{0:T(128)S(1)} %broadcast_multiply_fusion.1, bf16[1024,128]{0,1:T(8,128)(2,1)S(1)} %all_gather.7, f32[4,128]{1,0:T(4,128)S(1)} %get-tuple-element.44, f32[4,128]{1,0:T(4,128)S(1)} %get-tuple-element.43), kind=kOutput, calls=%fused_computation.19 | convolution fusion | flops 135987200 | bytes 2496528 | tf_op jit(solution)/shard_map/while/body/eval_jaxpr/kgqn,nkd->kgqd/dot_general | solution.py:107
  72.9 1.3 convolution_convert_fusion.1
  75.9 1.4 scatter_custom_fusion.1
  77.3 1.4 scatter_custom_fusion
  79.6 25.8 %all-reduce.2.cloned.1.call-done = bf16[128,2048]{1,0:T(8,128)(2,1)} async-done(((bf16[128,2048]{1,0:T(8,128)(2,1)}), bf16[128,2048]{1,0:T(8,128)(2,1)}) %all-reduce.2.cloned.1.call-update) | async-done | bytes 524304 | tf_op jit(solution)/shard_map/psum | solution.py:140
  105.4 1.3 multiply_reduce_fusion.1
  106.9 2.1 gather_fusion
  109.1 16.4 %all_to_all.15 = bf16[8,48,512]{2,1,0:T(8,128)(2,1)S(1)} all-to-all(bf16[8,48,512]{2,1,0:T(8,128)(2,1)S(1)} %broadcast_select_fusion), channel_id=1, replica_groups=mesh['sp'=8,'tp'=4] {'sp'}, dimensions={0} | all-to-all | bytes 786432 | tf_op jit(solution)/shard_map/all_to_all | solution.py:172
  125.7 22.5 %all_to_all.16 = bf16[4,8,48,512]{3,2,1,0:T(8,128)(2,1)S(1)} all-to-all(bf16[4,8,48,512]{3,2,1,0:T(8,128)(2,1)S(1)} %stack.2), channel_id=1, replica_groups=mesh['sp'=8,'tp'=4] {'tp'}, dimensions={0} | all-to-all | bytes 3145728 | tf_op jit(solution)/shard_map/all_to_all | solution.py:175
  148.2 1.2 copy.41
  149.9 1.1 copy-done.6
  151.0 1.0 fusion.3
  152.6 1.0 fusion.10
  153.6 2.1 %convolution_convert_fusion = bf16[8,48,2048]{2,1,0:T(8,128)(2,1)} fusion(bf16[8,48,512]{2,1,0:T(8,128)(2,1)S(1)} %bitcast.89, bf16[1,512,2048]{2,1,0:T(8,128)(2,1)S(1)} %copy-done), kind=kOutput, calls=%fused_computation.4 | convolution fusion | flops 806092800 | bytes 4063232 | tf_op jit(solution)/shard_map/dot_general | solution.py:182
  155.8 25.9 %reduce-scatter.2.cloned.1.call-done = bf16[8,48,512]{2,1,0:T(8,128)(2,1)} async-done(((bf16[8,48,2048]{2,1,0:T(8,128)(2,1)}), bf16[8,48,512]{2,1,0:T(8,128)(2,1)}) %reduce-scatter.2.cloned.1.call-update) | async-done | bytes 393232 | tf_op jit(solution)/shard_map/reduce_scatter | solution.py:184
  181.7 5.5 %all-to-all-start.2 = ((bf16[8,48,512]{2,1,0:T(8,128)(2,1)}), bf16[8,48,512]{2,1,0:T(8,128)(2,1)S(1)}, u32[]{:S(2)}, u32[]{:S(2)}) async-start(bf16[8,48,512]{2,1,0:T(8,128)(2,1)} %reduce-scatter.2.cloned.1.call-done), calls=%async_computation.3 | async-start | bytes 786432 | tf_op jit(solution)/shard_map/all_to_all | solution.py:187
  187.4 11.4 %all-to-all-done.2 = bf16[8,48,512]{2,1,0:T(8,128)(2,1)S(1)} async-done(((bf16[8,48,512]{2,1,0:T(8,128)(2,1)}), bf16[8,48,512]{2,1,0:T(8,128)(2,1)S(1)}, u32[]{:S(2)}, u32[]{:S(2)}) %all-to-all-start.2) | async-done | bytes 393248 | tf_op jit(solution)/shard_map/all_to_all | solution.py:187
  198.8 1.2 gather_fusion.1
  (72 shorter events, 10.8 us)
Async XLA Ops:
  6.5 147.1 %copy-start = (bf16[1,512,2048]{2,1,0:T(8,128)(2,1)S(1)}, bf16[1,512,2048]{2,1,0:T(8,128)(2,1)}, u32[]{:S(2)}) copy-start(bf16[1,512,2048]{2,1,0:T(8,128)(2,1)} %param.27) | copy-start | bytes 6291460
  6.5 98.8 %all-reduce.2.cloned.1.call-start = ((), (), s32[]{:S(2)}) async-start(), calls=%async_computation.4 | async-start | bytes 1048576 | tf_op jit(solution)/shard_map/psum | solution.py:140
  41.1 1.4 copy-start.1
  43.8 29.1 %copy-start.2 = (bf16[512,2048]{1,0:T(8,128)(2,1)S(1)}, bf16[512,2048]{1,0:T(8,128)(2,1)}, u32[]{:S(2)}) copy-start(bf16[512,2048]{1,0:T(8,128)(2,1)} %param.21) | copy-start | bytes 6291460
  72.9 1.4 copy-start.5
  72.9 32.5 %copy-start.3 = (bf16[128,2048]{1,0:T(8,128)(2,1)S(1)}, bf16[128,2048]{1,0:T(8,128)(2,1)}, u32[]{:S(2)}) copy-start(bf16[128,2048]{1,0:T(8,128)(2,1)} %param.14) | copy-start | bytes 1572868
  74.2 107.5 %reduce-scatter.2.cloned.1.call-start = ((), (), s32[]{:S(2)}) async-start(), calls=%async_computation.5 | async-start | bytes 1966080 | tf_op jit(solution)/shard_map/reduce_scatter | solution.py:184
  149.4 1.6 copy-start.6
  151.0 1.6 copy-start.7
  155.8 31.5 %copy-start.4 = (f32[128,2]{0,1:T(2,128)S(1)}, f32[128,2]{0,1:T(2,128)}, u32[]{:S(2)}) copy-start(f32[128,2]{0,1:T(2,128)} %param.23) | copy-start | bytes 3076
  181.7 17.1 %all-to-all-start.2 = ((bf16[8,48,512]{2,1,0:T(8,128)(2,1)}), bf16[8,48,512]{2,1,0:T(8,128)(2,1)S(1)}, u32[]{:S(2)}, u32[]{:S(2)}) async-start(bf16[8,48,512]{2,1,0:T(8,128)(2,1)} %reduce-scatter.2.cloned.1.call-done), calls=%async_computation.3 | async-start | bytes 786432 | tf_op jit(solution)/shard_map/all_to_all | solution.py:187
Sparse Core Ops, SparseCore 0:
  74.3 30.9 all-reduce.1
  155.9 25.7 reduce-scatter.1
